TPU v7x, 32 devices: a whole 2x2x4 slice. The times are simulated.
32 devices in a mesh: kv: 8 (over z, y), tp: 4 (over x, core).
Axes of the slice: x: 2, y: 2, z: 4, core: 2. Of those that a mesh axis runs over, the one named last changes fastest.
Arguments:
- hidden: bfloat16 [128, 4096], P(None, 'tp'), may hold values from -50 to 50
- input_gain: bfloat16 [4096], P('tp'), may hold values from 0.099609375 to 1.8984375
- x_weight: bfloat16 [4096, 8192], P('tp', 'kv'), may hold values from -0.09375 to 0.09375
- z_weight: bfloat16 [4096, 8192], P('tp', 'kv'), may hold values from -0.09375 to 0.09375
- bc_weight: bfloat16 [4096, 8192], P('tp', 'kv'), may hold values from -0.09375 to 0.09375
- dt_weight: bfloat16 [4096, 128], P('tp', 'kv'), may hold values from -0.09375 to 0.09375
- x_kernel: bfloat16 [4, 8192], P(None, 'kv'), may hold values from -3 to 3
- bc_kernel: bfloat16 [4, 8192], P(None, 'kv'), may hold values from -3 to 3
- dt_bias: float32 [128], P('kv'), may hold values from -3 to 0.5
- decay_log: float32 [128], P('kv'), may hold values from -3 to 1.5
- skip_scale: float32 [128], P('kv'), may hold values from 0.5 to 1.5
- output_gain: bfloat16 [8192], P('kv'), may hold values from 0.099609375 to 1.8984375
- output_weight: bfloat16 [8192, 4096], P('kv'), may hold values from -0.09375 to 0.09375
- saved_states: float32 [32, 5, 128, 64, 128], P('tp', None, 'kv'), may hold values from -1.8 to 1.8
- x_history: bfloat16 [32, 7, 8192], P('tp', None, 'kv'), may hold values from -6 to 6
- bc_history: bfloat16 [32, 7, 8192], P('tp', None, 'kv'), may hold values from -6 to 6
- accepted: int32 [32], P('tp'), may hold values from 0 to 4
Outputs:
- mixed: bfloat16 [128, 4096], P('tp', 'kv')
- new_states: float32 [32, 5, 128, 64, 128], P('tp', None, 'kv')
- x_window: bfloat16 [32, 7, 8192], P('tp', None, 'kv')
- bc_window: bfloat16 [32, 7, 8192], P('tp', None, 'kv')
All inputs are finite; a program needn't handle non-finite values.
Results may differ from a plain program's by a relative error of at most 0.02.
Values may be sent and summed in bfloat16 or wider, within the bound.
A program may use at most 192 MiB of HBM per device.

v0:
```python
import jax
import jax.numpy as jnp
from jax import lax
from jax.sharding import PartitionSpec as P

D = 4096
PROPS = 4
INNER = 8192
EPSILON = 1e-05


def partner_2(block, axis, stride):
    count = lax.axis_size(axis)
    route = []
    for low in range(count):
        high = low | 1 << stride
        if high != low and high < count:
            route += [(low, high), (high, low)]
    return lax.ppermute(block, axis, route)


def take_window(history, accepted, fresh_rows):
    history_len = history.shape[1] - fresh_rows.shape[1]
    indices = accepted[:, None] + jnp.arange(history_len, dtype=jnp.int32)[None, :]
    kept_rows = jnp.take_along_axis(history, indices[:, :, None], axis=1)
    return jnp.concatenate([kept_rows, fresh_rows], axis=1)


def conv_silu(window, kernel):
    length = window.shape[1] - kernel.shape[0] + 1
    running = window[:, 0:length].astype(jnp.float32) * kernel[0].astype(jnp.float32)
    for offset in range(1, kernel.shape[0]):
        running = running + window[:, offset : offset + length].astype(jnp.float32) * kernel[
            offset
        ].astype(jnp.float32)
    return jax.nn.silu(running)


def ssd_block(x_conv, step_size, decay_rate, b_terms, c_terms, first_state, skip_scale):
    cumulated = jnp.cumsum(-decay_rate * step_size, axis=1)
    length = x_conv.shape[1]
    indices = jnp.arange(length)
    causal = indices[:, None] >= indices[None, :]
    gaps = cumulated[:, :, None, :] - cumulated[:, None, :, :]
    weights = jnp.exp(jnp.where(causal[None, :, :, None], gaps, -jnp.inf))
    inputs = x_conv * step_size[..., None]
    outer_prod = jnp.einsum("srhp,srhn->srhpn", inputs, b_terms)
    states = jnp.exp(cumulated)[..., None, None] * first_state[:, None] + jnp.einsum(
        "strh,srhpn->sthpn", weights, outer_prod
    )
    output = jnp.einsum("sthn,sthpn->sthp", c_terms, states) + skip_scale[:, None] * x_conv
    return (output, states)


def local(
    hidden,
    input_gain,
    x_weight,
    z_weight,
    bc_weight,
    dt_weight,
    x_kernel,
    bc_kernel,
    dt_bias,
    decay_log,
    skip_scale,
    output_gain,
    output_weight,
    saved_states,
    x_history,
    bc_history,
    accepted,
):
    heads_here = dt_bias.shape[0]
    head_size = x_weight.shape[1] // heads_here
    state_size = saved_states.shape[4]
    seqs_here = accepted.shape[0]
    rows_here = hidden.shape[0] // lax.axis_size("tp")
    inner_here = x_weight.shape[1]
    bc_here = bc_weight.shape[1]
    widened = hidden.astype(jnp.float32)
    squares = lax.psum(jnp.sum(widened * widened, axis=1), "tp")
    normed = (
        widened * lax.rsqrt(squares[:, None] / D + EPSILON) * input_gain.astype(jnp.float32)
    ).astype(jnp.bfloat16)
    weights = jnp.concatenate([x_weight, z_weight, bc_weight, dt_weight], axis=1)
    product = jnp.dot(normed, weights, preferred_element_type=jnp.float32)
    projected = lax.psum_scatter(
        lax.optimization_barrier(product.astype(jnp.bfloat16))
        .astype(jnp.float32)
        .astype(jnp.bfloat16),
        "tp",
        scatter_dimension=0,
        tiled=True,
    )
    x_fresh = projected[:, :inner_here]
    z_fresh = projected[:, inner_here : 2 * inner_here]
    bc_fresh = projected[:, 2 * inner_here : 2 * inner_here + bc_here]
    dt_fresh = projected[:, 2 * inner_here + bc_here :]
    x_window = take_window(x_history, accepted, x_fresh.reshape(seqs_here, PROPS, inner_here))
    bc_window = take_window(bc_history, accepted, bc_fresh.reshape(seqs_here, PROPS, bc_here))
    x_conv = conv_silu(x_window, x_kernel).reshape(seqs_here, PROPS, heads_here, head_size)
    bc_conv = conv_silu(bc_window, bc_kernel)
    spread = max(4 // heads_here, 1)
    position = lax.axis_index("kv")
    for level in range(spread.bit_length() - 1):
        partner = partner_2(bc_conv, "kv", level)
        low_half = position // 2**level % 2 == 0
        bc_conv = jnp.where(
            low_half,
            jnp.concatenate([bc_conv, partner], axis=2),
            jnp.concatenate([partner, bc_conv], axis=2),
        )
    groups_here = bc_conv.shape[2] // (2 * state_size)
    paired = bc_conv.reshape(seqs_here, PROPS, groups_here, 2, state_size)
    per_group = heads_here // groups_here
    b_terms = jnp.repeat(paired[:, :, :, 0], per_group, axis=2)
    c_terms = jnp.repeat(paired[:, :, :, 1], per_group, axis=2)
    step_size = jax.nn.softplus(
        dt_fresh.astype(jnp.float32).reshape(seqs_here, PROPS, heads_here) + dt_bias
    )
    first_state = jnp.take_along_axis(saved_states, accepted[:, None, None, None, None], axis=1)[
        :, 0
    ]
    output, states = ssd_block(
        x_conv, step_size, jnp.exp(decay_log), b_terms, c_terms, first_state, skip_scale
    )
    new_states = jnp.concatenate([first_state[:, None], states], axis=1)
    gate_values = z_fresh.astype(jnp.float32).reshape(seqs_here, PROPS, heads_here, head_size)
    gated = (output * jax.nn.silu(gate_values)).reshape(rows_here, inner_here)
    square_sum = jnp.sum(gated * gated, axis=1)
    scaled = (gated * output_gain.astype(jnp.float32)).astype(jnp.bfloat16)
    partial_value = jnp.dot(scaled, output_weight, preferred_element_type=jnp.float32)
    total_squares = lax.psum(square_sum, "kv")
    summed = lax.psum_scatter(partial_value, "kv", scatter_dimension=1, tiled=True)
    mixed = (lax.rsqrt(total_squares / INNER + EPSILON)[:, None] * summed).astype(jnp.bfloat16)
    return (mixed, new_states, x_window, bc_window)


def solution(mesh):
    in_specs = (
        P(None, "tp"),
        P("tp"),
        P("tp", "kv"),
        P("tp", "kv"),
        P("tp", "kv"),
        P("tp", "kv"),
        P(None, "kv"),
        P(None, "kv"),
        P("kv"),
        P("kv"),
        P("kv"),
        P("kv"),
        P("kv", None),
        P("tp", None, "kv", None, None),
        P("tp", None, "kv"),
        P("tp", None, "kv"),
        P("tp"),
    )
    out_specs = (
        P("tp", "kv"),
        P("tp", None, "kv", None, None),
        P("tp", None, "kv"),
        P("tp", None, "kv"),
    )
    return jax.shard_map(local, mesh=mesh, in_specs=in_specs, out_specs=out_specs, check_vma=False)
```

profile of v0, /device:TPU:0, one launch (start us, length us, event | category | flops | bytes accessed | tf_op | source)
XLA Modules:
  0.0 164.1 jit_solution(15969078561055886669)
XLA Ops:
  7.2 1.1 fusion.19
  8.3 8.4 %psum.14 = f32[128]{0:T(128)S(1)} all-reduce(f32[128]{0:T(128)S(1)} %fusion.19), channel_id=1, replica_groups=mesh['kv'=8,'tp'=4] {'tp'}, use_global_device_ids=true, to_apply=%region_1.3 | all-reduce | flops 128 | bytes 1024 | tf_op jit(solution)/shard_map/psum | solution.py:82
  17.4 0.9 copy.75
  18.4 5.7 %fusion.16 = bf16[128,3088]{0,1:T(8,128)(2,1)S(1)} fusion(bf16[1024,16]{1,0:T(8,128)(2,1)S(1)} %copy.75, bf16[1024,1024]{1,0:T(8,128)(2,1)} %param.23, bf16[1024,1024]{1,0:T(8,128)(2,1)} %param.22, bf16[1024,1024]{1,0:T(8,128)(2,1)} %param.21, bf16[128,1024]{1,0:T(8,128)(2,1)} %param.19, f32[1024]{0:T(1024)S(1)} %convert_element_type.130, ...), kind=kOutput, calls=%fused_computation.20 | convolution fusion | flops 835717120 | bytes 7381504 | tf_op jit(solution)/shard_map/dot_general | solution.py:87
  24.1 1.7 %copy.94 = bf16[128,3088]{1,0:T(8,128)(2,1)} copy(bf16[128,3088]{0,1:T(8,128)(2,1)S(1)} %fusion.16) | data formatting | bytes 1581056
  26.4 0.9 gather_fusion.2
  27.3 0.9 gather_fusion.1
  28.2 10.2 %gather_fusion = f32[8,16,64,128]{3,2,1,0:T(8,128)} fusion(f32[8,5,16,64,128]{4,3,2,1,0:T(8,128)} %param.32, s32[8]{0:T(128)S(1)} %or_bitcast_fusion), kind=kCustom, calls=%fused_computation.2 | custom fusion | bytes 8388672 | tf_op jit(solution)/shard_map/jit(take_along_axis)/gather | solution.py:122
  38.6 5.2 %broadcast_select_fusion.1 = f32[8,16,64,128]{3,2,1,0:T(8,128)} fusion(f32[8,16,64,128]{3,2,1,0:T(8,128)} %gather_fusion, pred[8]{0:T(512)(128)(4,1)S(1)} %compare_and_fusion), kind=kLoop, calls=%fused_computation.21 | loop fusion | flops 1048576 | bytes 8388616 | tf_op jit(solution)/shard_map/jit(take_along_axis)/select_n | solution.py:122
  43.8 6.5 %broadcast_select_fusion = f32[8,1,16,64,128]{4,1,3,2,0:T(1,128)} fusion(f32[8,1,16,64,128]{4,1,3,2,0:T(1,128)S(1)} %bitcast.44, pred[8]{0:T(512)(128)(4,1)S(1)} %compare_and_fusion), kind=kLoop, calls=%fused_computation.11 | loop fusion | flops 1048576 | bytes 8388616 | tf_op jit(solution)/shard_map/jit(take_along_axis)/select_n | solution.py:122
  51.3 0.9 fusion.54
  52.5 0.7 copy.89
  53.2 0.7 copy.88
  55.1 2.9 %copy.82 = f32[8,4,16,64]{1,3,2,0:T(8,128)} copy(f32[8,4,16,64]{3,2,1,0:T(8,128)S(1)} %broadcast_multiply_fusion) | data formatting | bytes 262144 | tf_op jit(solution)/shard_map/mul | solution.py:46
  58.0 15.6 %bitcast_add_fusion = f32[8,4,16,64,128]{4,1,3,2,0:T(4,128)S(1)} fusion(f32[8,4,16,128]{3,1,2,0:T(4,128)S(1)} %bitcast.45, f32[8,4,16,64]{1,3,2,0:T(8,128)} %copy.82, f32[8,16,64,128]{3,2,1,0:T(8,128)} %broadcast_select_fusion.1, f32[8,4,16]{1,2,0:T(8,128)S(1)} %copy.78, f32[8,4,16]{1,2,0:T(8,128)S(1)} %copy.84, pred[4,4]{1,0:T(4,128)(4,1)S(1)} %iota_compare_fusion), kind=kOutput, calls=%fused_computation.4 | convolution fusion | flops 46141440 | bytes 21368848 | tf_op jit(solution)/shard_map/strh,srhpn->sthpn/dot_general | solution.py:48
  73.8 6.1 %copy-done.3 = f32[8,4,16,64,128]{4,1,3,2,0:T(4,128)} copy-done((f32[8,4,16,64,128]{4,1,3,2,0:T(4,128)}, f32[8,4,16,64,128]{4,1,3,2,0:T(4,128)S(1)}, u32[]{:S(2)}) %copy-start.3) | copy-done | bytes 16777240
  79.8 5.1 %fusion = f32[8,4,16,1,64]{4,3,2,1,0:T(1,128)} fusion(f32[8,4,16,128,1]{3,4,2,1,0:T(1,128)S(1)} %bitcast.46, f32[8,4,16,64,128]{4,1,3,2,0:T(4,128)S(1)} %bitcast_add_fusion), kind=kOutput, calls=%fused_computation.5 | convolution fusion | flops 8388608 | bytes 17170432 | tf_op jit(solution)/shard_map/sthn,sthpn->sthp/dot_general | solution.py:51
  85.0 1.2 multiply_reduce_fusion
  86.4 5.7 %fusion.33 = f32[32,4096]{1,0:T(8,128)} fusion(bf16[1024,4096]{1,0:T(8,128)(2,1)} %param.31, f32[32,1024]{1,0:T(8,128)S(1)} %reshape.214, f32[1024]{0:T(1024)S(1)} %convert_element_type.157), kind=kOutput, calls=%fused_computation.57 | convolution fusion | flops 268500992 | bytes 9048064 | tf_op jit(solution)/shard_map/dot_general | solution.py:133
  92.2 20.0 %pad_maximum_fusion = f32[8,5,16,64,128]{4,1,3,2,0:T(8,128)} fusion(f32[8,4,16,64,128]{4,1,3,2,0:T(4,128)} %copy-done.3, f32[8,1,16,64,128]{4,1,3,2,0:T(1,128)} %broadcast_select_fusion), kind=kLoop, calls=%fused_computation.3 | loop fusion | flops 5242880 | bytes 41943040 | tf_op jit(solution)/shard_map/concatenate | solution.py:128
  112.2 19.5 %copy.87 = f32[8,5,16,64,128]{4,3,2,1,0:T(8,128)} copy(f32[8,5,16,64,128]{4,1,3,2,0:T(8,128)} %pad_maximum_fusion) | data formatting | bytes 41943040
  131.6 21.9 %psum.15 = f32[32]{0:T(128)S(1)} all-reduce(f32[32]{0:T(128)S(1)} %reduce_sum.22), channel_id=1, replica_groups=mesh['kv'=8,'tp'=4] {'kv'}, use_global_device_ids=true, to_apply=%region_5.7 | all-reduce | flops 32 | bytes 256 | tf_op jit(solution)/shard_map/psum | solution.py:134
  153.5 2.3 %reduce-scatter.5.cloned.1.call-done = f32[32,512]{1,0:T(8,128)} async-done(((f32[32,4096]{1,0:T(8,128)}), f32[32,512]{1,0:T(8,128)}) %reduce-scatter.5.cloned.1.call-update) | async-done | bytes 65552 | tf_op jit(solution)/shard_map/reduce_scatter | solution.py:135
  155.8 1.5 multiply_convert_fusion.2
  (69 shorter events, 4.1 us)
Async XLA Ops:
  7.2 19.2 %copy-start = (bf16[8,7,1024]{2,0,1:T(8,128)(2,1)S(1)}, bf16[8,7,1024]{2,0,1:T(8,128)(2,1)}, u32[]{:S(2)}) copy-start(bf16[8,7,1024]{2,0,1:T(8,128)(2,1)} %param.33) | copy-start | bytes 344068
  7.2 43.1 %reduce-scatter.7.cloned.1.call-start = ((), (), s32[]{:S(2)}) async-start(), calls=%async_computation.3 | async-start | bytes 1024000 | tf_op jit(solution)/shard_map/reduce_scatter | solution.py:88
  18.3 7.6 %copy-start.10 = (s32[8]{0:T(128)S(1)}, s32[8]{0:T(128)}, u32[]{:S(2)}) copy-start(s32[8]{0:T(128)} %param.35) | copy-start | bytes 100
  18.3 7.6 %copy-start.11 = (f32[16]{0:T(128)S(1)}, f32[16]{0:T(128)}, u32[]{:S(2)}) copy-start(f32[16]{0:T(128)} %param.28) | copy-start | bytes 196
  18.3 7.7 %copy-start.5 = (bf16[4,1024]{1,0:T(4,128)(2,1)S(1)}, bf16[4,1024]{1,0:T(4,128)(2,1)}, u32[]{:S(2)}) copy-start(bf16[4,1024]{1,0:T(4,128)(2,1)} %param.25) | copy-start | bytes 24580
  18.4 7.7 %copy-start.6 = (bf16[4,1024]{1,0:T(4,128)(2,1)S(1)}, bf16[4,1024]{1,0:T(4,128)(2,1)}, u32[]{:S(2)}) copy-start(bf16[4,1024]{1,0:T(4,128)(2,1)} %param.26) | copy-start | bytes 24580
  18.4 8.0 %copy-start.7 = (bf16[1024]{0:T(1024)(128)(2,1)S(1)}, bf16[1024]{0:T(1024)(128)(2,1)}, u32[]{:S(2)}) copy-start(bf16[1024]{0:T(1024)(128)(2,1)} %param.30) | copy-start | bytes 6148
  18.4 8.9 %copy-start.4 = (bf16[8,7,1024]{2,0,1:T(8,128)(2,1)S(1)}, bf16[8,7,1024]{2,0,1:T(8,128)(2,1)}, u32[]{:S(2)}) copy-start(bf16[8,7,1024]{2,0,1:T(8,128)(2,1)} %param.34) | copy-start | bytes 344068
  25.8 130.0 %reduce-scatter.5.cloned.1.call-start = ((), (), s32[]{:S(2)}) async-start(), calls=%async_computation.2 | async-start | bytes 589824 | tf_op jit(solution)/shard_map/reduce_scatter | solution.py:135
  38.4 5.3 %copy-start.2 = (f32[8,16,64,128]{3,2,1,0:T(8,128)S(1)}, f32[8,16,64,128]{3,2,1,0:T(8,128)}, u32[]{:S(2)}) copy-start(f32[8,16,64,128]{3,2,1,0:T(8,128)} %gather_fusion) | copy-start | bytes 12582916
  38.6 12.4 %copy-start.8 = (f32[16]{0:T(128)S(1)}, f32[16]{0:T(128)}, u32[]{:S(2)}) copy-start(f32[16]{0:T(128)} %param.27) | copy-start | bytes 196
  73.7 6.2 %copy-start.3 = (f32[8,4,16,64,128]{4,1,3,2,0:T(4,128)}, f32[8,4,16,64,128]{4,1,3,2,0:T(4,128)S(1)}, u32[]{:S(2)}) copy-start(f32[8,4,16,64,128]{4,1,3,2,0:T(4,128)S(1)} %bitcast_add_fusion) | copy-start | bytes 50331652
  73.7 11.3 %copy-start.9 = (f32[16]{0:T(128)S(1)}, f32[16]{0:T(128)}, u32[]{:S(2)}) copy-start(f32[16]{0:T(128)} %param.29) | copy-start | bytes 196
  112.2 45.1 %copy-start.1 = (bf16[8,7,1024]{2,0,1:T(8,128)(2,1)S(1)}, bf16[8,7,1024]{2,0,1:T(8,128)(2,1)}, u32[]{:S(2)}) copy-start(bf16[8,7,1024]{2,0,1:T(8,128)(2,1)} %param.33) | copy-start | bytes 344068
Sparse Core Ops, SparseCore 0:
  25.9 23.7 reduce-scatter.6
  92.3 63.4 reduce-scatter.4
where the time goes:
time: 165 us; the launch traced here: 164 us
  local copies, waits for them, and re-layouts  46.8 us (28%)
  other arithmetic  38.2 us (23%)
  matrix products  32.2 us (20%)
  blocking collectives  30.2 us (18%)
  between operations  14.4 us (9%)
  waiting for transfers between devices  2.31 us (1%)
    unnamed x30, local copies, waits for them, and re-layouts  29.7 us
    psum x1, blocking collectives, local(): total_squares = lax.psum(square_sum, 'kv')  21.9 us
    concatenate x1, other arithmetic, local(): new_states = jnp.concatenate([first_state[:, None], states], axis=1)  20 us
    dot_general x1, matrix products, ssd_block(): jnp.einsum('strh,srhpn->sthpn', weights, outer_prod)  15.6 us
    select_n x2, other arithmetic, local(): jnp.take_along_axis(saved_states, accepted[:, None, None, None, None], ax...  11.7 us
    gather x1, local copies, waits for them, and re-layouts, local(): jnp.take_along_axis(saved_states, accepted[:, None, None, None, None], ax...  10.2 us
    psum x1, blocking collectives, local(): squares = lax.psum(jnp.sum(widened * widened, axis=1), 'tp')  8.36 us
    dot_general x1, matrix products, local(): jnp.dot(scaled, output_weight, preferred_element_type=jnp.float32)  5.75 us
  transfers between devices with their start and end apart: 2, of which 1 were waited for; matrix products, arithmetic and copies ran while one was open for 39% of the time, Pallas kernels for 0%

commit v1 on v0

--- a/solution.py
+++ b/solution.py
@@ -79,7 +79,7 @@
     inner_here = x_weight.shape[1]
     bc_here = bc_weight.shape[1]
     widened = hidden.astype(jnp.float32)
-    squares = lax.psum(jnp.sum(widened * widened, axis=1), "tp")
+    squares = jnp.sum(lax.all_gather(jnp.sum(widened * widened, axis=1), "tp"), axis=0)
     normed = (
         widened * lax.rsqrt(squares[:, None] / D + EPSILON) * input_gain.astype(jnp.float32)
     ).astype(jnp.bfloat16)

time: 165 us -> 164 us (level)
  blocking collectives: 30.2 us -> 27.4 us
  waiting for transfers between devices: 2.31 us -> 4.43 us
    psum x1 -> x0, blocking collectives: 8.36 us -> none  [local(): squares = lax.psum(jnp.sum(widened * widened, axis=1), 'tp')]
    all_gather x0 -> x1, blocking collectives: none -> 6 us  [local(): lax.all_gather(jnp.sum(widened * widened, axis=1), 'tp')]
  transfers between devices with their start and end apart: 2 -> 2, of which waited for: 1 -> 2; matrix products, arithmetic and copies ran while one was open for 39% -> 39% of each run, Pallas kernels for 0% -> 0%
where the time goes in v1:
time: 164 us; the launch traced here: 163 us
  local copies, waits for them, and re-layouts  46.6 us (28%)
  other arithmetic  38.2 us (23%)
  matrix products  32.2 us (20%)
  blocking collectives  27.4 us (17%)
  between operations  14.4 us (9%)
  waiting for transfers between devices  4.43 us (3%)
    unnamed x30, local copies, waits for them, and re-layouts  29.7 us
    psum x1, blocking collectives, local(): total_squares = lax.psum(square_sum, 'kv')  21.4 us
    concatenate x1, other arithmetic, local(): new_states = jnp.concatenate([first_state[:, None], states], axis=1)  20 us
    dot_general x1, matrix products, ssd_block(): jnp.einsum('strh,srhpn->sthpn', weights, outer_prod)  15.6 us
    select_n x2, other arithmetic, local(): jnp.take_along_axis(saved_states, accepted[:, None, None, None, None], ax...  11.7 us
    gather x1, local copies, waits for them, and re-layouts, local(): jnp.take_along_axis(saved_states, accepted[:, None, None, None, None], ax...  10.1 us
    all_gather x1, blocking collectives, local(): lax.all_gather(jnp.sum(widened * widened, axis=1), 'tp')  6 us
    dot_general x1, matrix products, local(): jnp.dot(scaled, output_weight, preferred_element_type=jnp.float32)  5.75 us
  transfers between devices with their start and end apart: 2, of which 2 were waited for; matrix products, arithmetic and copies ran while one was open for 39% of the time, Pallas kernels for 0%

profile of v1, /device:TPU:0, one launch (start us, length us, event | category | flops | bytes accessed | tf_op | source)
XLA Modules:
  0.0 163.3 jit_solution(3840665118973975195)
XLA Ops:
  7.2 1.1 fusion.19
  8.3 6.0 %all-gather.1 = f32[4,1,128]{2,1,0:T(1,128)S(1)} all-gather(f32[1,1,128]{2,1,0:T(1,128)S(1)} %bitcast.60), channel_id=2, replica_groups=mesh['kv'=8,'tp'=4] {'tp'}, dimensions={0}, use_global_device_ids=true | all-gather | bytes 2560 | tf_op jit(solution)/shard_map/all_gather | solution.py:82
  15.0 0.9 copy.75
  16.1 5.7 %fusion.16 = bf16[128,3088]{0,1:T(8,128)(2,1)S(1)} fusion(bf16[1024,16]{1,0:T(8,128)(2,1)S(1)} %copy.75, bf16[1024,1024]{1,0:T(8,128)(2,1)} %param.23, bf16[1024,1024]{1,0:T(8,128)(2,1)} %param.22, bf16[1024,1024]{1,0:T(8,128)(2,1)} %param.21, bf16[128,1024]{1,0:T(8,128)(2,1)} %param.19, f32[1024]{0:T(1024)S(1)} %convert_element_type.130, ...), kind=kOutput, calls=%fused_computation.20 | convolution fusion | flops 835717120 | bytes 7381504 | tf_op jit(solution)/shard_map/dot_general | solution.py:87
  21.7 1.7 %copy.94 = bf16[128,3088]{1,0:T(8,128)(2,1)} copy(bf16[128,3088]{0,1:T(8,128)(2,1)S(1)} %fusion.16) | data formatting | bytes 1581056
  24.0 0.9 gather_fusion.2
  25.0 0.9 gather_fusion.1
  25.9 10.1 %gather_fusion = f32[8,16,64,128]{3,2,1,0:T(8,128)} fusion(f32[8,5,16,64,128]{4,3,2,1,0:T(8,128)} %param.32, s32[8]{0:T(128)S(1)} %or_bitcast_fusion), kind=kCustom, calls=%fused_computation.2 | custom fusion | bytes 8388672 | tf_op jit(solution)/shard_map/jit(take_along_axis)/gather | solution.py:122
  36.1 5.2 %broadcast_select_fusion.1 = f32[8,16,64,128]{3,2,1,0:T(8,128)} fusion(f32[8,16,64,128]{3,2,1,0:T(8,128)} %gather_fusion, pred[8]{0:T(512)(128)(4,1)S(1)} %compare_and_fusion), kind=kLoop, calls=%fused_computation.21 | loop fusion | flops 1048576 | bytes 8388616 | tf_op jit(solution)/shard_map/jit(take_along_axis)/select_n | solution.py:122
  41.3 6.5 %broadcast_select_fusion = f32[8,1,16,64,128]{4,1,3,2,0:T(1,128)} fusion(f32[8,1,16,64,128]{4,1,3,2,0:T(1,128)S(1)} %bitcast.45, pred[8]{0:T(512)(128)(4,1)S(1)} %compare_and_fusion), kind=kLoop, calls=%fused_computation.11 | loop fusion | flops 1048576 | bytes 8388616 | tf_op jit(solution)/shard_map/jit(take_along_axis)/select_n | solution.py:122
  47.8 1.1 reduce-scatter.7.cloned.1.call-done
  49.9 0.9 fusion.54
  51.0 0.7 copy.89
  53.7 2.9 %copy.82 = f32[8,4,16,64]{1,3,2,0:T(8,128)} copy(f32[8,4,16,64]{3,2,1,0:T(8,128)S(1)} %broadcast_multiply_fusion) | data formatting | bytes 262144 | tf_op jit(solution)/shard_map/mul | solution.py:46
  56.6 15.6 %bitcast_add_fusion = f32[8,4,16,64,128]{4,1,3,2,0:T(4,128)S(1)} fusion(f32[8,4,16,128]{3,1,2,0:T(4,128)S(1)} %bitcast.46, f32[8,4,16,64]{1,3,2,0:T(8,128)} %copy.82, f32[8,16,64,128]{3,2,1,0:T(8,128)} %broadcast_select_fusion.1, f32[8,4,16]{1,2,0:T(8,128)S(1)} %copy.78, f32[8,4,16]{1,2,0:T(8,128)S(1)} %copy.84, pred[4,4]{1,0:T(4,128)(4,1)S(1)} %iota_compare_fusion), kind=kOutput, calls=%fused_computation.4 | convolution fusion | flops 46141440 | bytes 21368848 | tf_op jit(solution)/shard_map/strh,srhpn->sthpn/dot_general | solution.py:48
  72.3 6.1 %copy-done.3 = f32[8,4,16,64,128]{4,1,3,2,0:T(4,128)} copy-done((f32[8,4,16,64,128]{4,1,3,2,0:T(4,128)}, f32[8,4,16,64,128]{4,1,3,2,0:T(4,128)S(1)}, u32[]{:S(2)}) %copy-start.3) | copy-done | bytes 16777240
  78.4 5.1 %fusion = f32[8,4,16,1,64]{4,3,2,1,0:T(1,128)} fusion(f32[8,4,16,128,1]{3,4,2,1,0:T(1,128)S(1)} %bitcast.47, f32[8,4,16,64,128]{4,1,3,2,0:T(4,128)S(1)} %bitcast_add_fusion), kind=kOutput, calls=%fused_computation.5 | convolution fusion | flops 8388608 | bytes 17170432 | tf_op jit(solution)/shard_map/sthn,sthpn->sthp/dot_general | solution.py:51
  83.5 1.2 multiply_reduce_fusion
  85.0 5.7 %fusion.33 = f32[32,4096]{1,0:T(8,128)} fusion(bf16[1024,4096]{1,0:T(8,128)(2,1)} %param.31, f32[32,1024]{1,0:T(8,128)S(1)} %reshape.218, f32[1024]{0:T(1024)S(1)} %convert_element_type.157), kind=kOutput, calls=%fused_computation.57 | convolution fusion | flops 268500992 | bytes 9048064 | tf_op jit(solution)/shard_map/dot_general | solution.py:133
  90.7 20.0 %pad_maximum_fusion = f32[8,5,16,64,128]{4,1,3,2,0:T(8,128)} fusion(f32[8,4,16,64,128]{4,1,3,2,0:T(4,128)} %copy-done.3, f32[8,1,16,64,128]{4,1,3,2,0:T(1,128)} %broadcast_select_fusion), kind=kLoop, calls=%fused_computation.3 | loop fusion | flops 5242880 | bytes 41943040 | tf_op jit(solution)/shard_map/concatenate | solution.py:128
  110.7 19.5 %copy.87 = f32[8,5,16,64,128]{4,3,2,1,0:T(8,128)} copy(f32[8,5,16,64,128]{4,1,3,2,0:T(8,128)} %pad_maximum_fusion) | data formatting | bytes 41943040
  130.2 21.4 %psum.7 = f32[32]{0:T(128)S(1)} all-reduce(f32[32]{0:T(128)S(1)} %reduce_sum.32), channel_id=1, replica_groups=mesh['kv'=8,'tp'=4] {'kv'}, use_global_device_ids=true, to_apply=%region_5.7 | all-reduce | flops 32 | bytes 256 | tf_op jit(solution)/shard_map/psum | solution.py:134
  151.6 3.3 %reduce-scatter.5.cloned.1.call-done = f32[32,512]{1,0:T(8,128)} async-done(((f32[32,4096]{1,0:T(8,128)}), f32[32,512]{1,0:T(8,128)}) %reduce-scatter.5.cloned.1.call-update) | async-done | bytes 65552 | tf_op jit(solution)/shard_map/reduce_scatter | solution.py:135
  154.9 1.5 multiply_convert_fusion.2
  (70 shorter events, 4.9 us)
Async XLA Ops:
  7.2 16.8 %copy-start = (bf16[8,7,1024]{2,0,1:T(8,128)(2,1)S(1)}, bf16[8,7,1024]{2,0,1:T(8,128)(2,1)}, u32[]{:S(2)}) copy-start(bf16[8,7,1024]{2,0,1:T(8,128)(2,1)} %param.33) | copy-start | bytes 344068
  7.2 41.7 %reduce-scatter.7.cloned.1.call-start = ((), (), s32[]{:S(2)}) async-start(), calls=%async_computation.3 | async-start | bytes 1024000 | tf_op jit(solution)/shard_map/reduce_scatter | solution.py:88
  16.0 7.6 %copy-start.10 = (s32[8]{0:T(128)S(1)}, s32[8]{0:T(128)}, u32[]{:S(2)}) copy-start(s32[8]{0:T(128)} %param.35) | copy-start | bytes 100
  16.0 7.6 %copy-start.11 = (f32[16]{0:T(128)S(1)}, f32[16]{0:T(128)}, u32[]{:S(2)}) copy-start(f32[16]{0:T(128)} %param.28) | copy-start | bytes 196
  16.0 7.7 %copy-start.5 = (bf16[4,1024]{1,0:T(4,128)(2,1)S(1)}, bf16[4,1024]{1,0:T(4,128)(2,1)}, u32[]{:S(2)}) copy-start(bf16[4,1024]{1,0:T(4,128)(2,1)} %param.25) | copy-start | bytes 24580
  16.0 7.7 %copy-start.6 = (bf16[4,1024]{1,0:T(4,128)(2,1)S(1)}, bf16[4,1024]{1,0:T(4,128)(2,1)}, u32[]{:S(2)}) copy-start(bf16[4,1024]{1,0:T(4,128)(2,1)} %param.26) | copy-start | bytes 24580
  16.0 8.0 %copy-start.7 = (bf16[1024]{0:T(1024)(128)(2,1)S(1)}, bf16[1024]{0:T(1024)(128)(2,1)}, u32[]{:S(2)}) copy-start(bf16[1024]{0:T(1024)(128)(2,1)} %param.30) | copy-start | bytes 6148
  16.0 8.9 %copy-start.4 = (bf16[8,7,1024]{2,0,1:T(8,128)(2,1)S(1)}, bf16[8,7,1024]{2,0,1:T(8,128)(2,1)}, u32[]{:S(2)}) copy-start(bf16[8,7,1024]{2,0,1:T(8,128)(2,1)} %param.34) | copy-start | bytes 344068
  23.5 131.4 %reduce-scatter.5.cloned.1.call-start = ((), (), s32[]{:S(2)}) async-start(), calls=%async_computation.2 | async-start | bytes 589824 | tf_op jit(solution)/shard_map/reduce_scatter | solution.py:135
  35.9 5.3 %copy-start.2 = (f32[8,16,64,128]{3,2,1,0:T(8,128)S(1)}, f32[8,16,64,128]{3,2,1,0:T(8,128)}, u32[]{:S(2)}) copy-start(f32[8,16,64,128]{3,2,1,0:T(8,128)} %gather_fusion) | copy-start | bytes 12582916
  36.1 13.5 %copy-start.8 = (f32[16]{0:T(128)S(1)}, f32[16]{0:T(128)}, u32[]{:S(2)}) copy-start(f32[16]{0:T(128)} %param.27) | copy-start | bytes 196
  72.2 6.2 %copy-start.3 = (f32[8,4,16,64,128]{4,1,3,2,0:T(4,128)}, f32[8,4,16,64,128]{4,1,3,2,0:T(4,128)S(1)}, u32[]{:S(2)}) copy-start(f32[8,4,16,64,128]{4,1,3,2,0:T(4,128)S(1)} %bitcast_add_fusion) | copy-start | bytes 50331652
  72.3 11.3 %copy-start.9 = (f32[16]{0:T(128)S(1)}, f32[16]{0:T(128)}, u32[]{:S(2)}) copy-start(f32[16]{0:T(128)} %param.29) | copy-start | bytes 196
  110.7 45.7 %copy-start.1 = (bf16[8,7,1024]{2,0,1:T(8,128)(2,1)S(1)}, bf16[8,7,1024]{2,0,1:T(8,128)(2,1)}, u32[]{:S(2)}) copy-start(bf16[8,7,1024]{2,0,1:T(8,128)(2,1)} %param.33) | copy-start | bytes 344068
Sparse Core Ops, SparseCore 0:
  23.6 25.1 reduce-scatter.6
  90.8 63.9 reduce-scatter.4
